TPU v7x, 32 devices: a whole 2x2x4 slice. The times are simulated.
32 devices in a mesh: ep: 8 (over z, x), tp: 4 (over y, core).
Axes of the slice: x: 2, y: 2, z: 4, core: 2. Of those that a mesh axis runs over, the one named last changes fastest.
Arguments:
- mixer_input: bfloat16 [2048, 2048], P('ep', 'tp'), may hold values from -80 to 80
- mixer_gain: float32 [2048], P('tp'), may hold values from 0.1 to 1.9
- time_step: float32 [2048, 128], P('ep', 'tp'), may hold values from 0.25 to 4
- pole_real: float32 [128, 32], P('tp'), may hold values from -0.1 to 0, as said below
- pole_imag: float32 [128, 32], P('tp'), may hold values from 0.25 to 3
- input_real: float32 [128, 32, 16], P('tp'), may hold values from -1 to 1
- input_imag: float32 [128, 32, 16], P('tp'), may hold values from -1 to 1
- read_real: float32 [128, 16, 32], P('tp'), may hold values from -1 to 1
- read_imag: float32 [128, 16, 32], P('tp'), may hold values from -1 to 1
- out_value: bfloat16 [2048, 2048], P(None, 'tp'), may hold values from -0.125 to 0.125
- out_gate: bfloat16 [2048, 2048], P(None, 'tp'), may hold values from -0.125 to 0.125
- expert_input: bfloat16 [1024, 2048], P('ep', 'tp'), may hold values from -80 to 80
- expert_gain: float32 [2048], P('tp'), may hold values from 0.1 to 1.9
- routes: int32 [1024, 2], P('ep'), may hold values from 0 to 7, all different within a row; in each aligned block of 128 rows (0 to 127, 128 to 255, ...) at most 64 rows name the same one
- route_weight: float32 [1024, 2], P('ep'), may hold values from 0.2 to 1
- expert_gate: bfloat16 [8, 2048, 4096], P('ep', None, 'tp'), may hold values from -0.125 to 0.125
- expert_up: bfloat16 [8, 2048, 4096], P('ep', None, 'tp'), may hold values from -0.125 to 0.125
- expert_down: bfloat16 [8, 4096, 2048], P('ep', 'tp'), may hold values from -0.125 to 0.125
Outputs:
- mixer_output: bfloat16 [2048, 2048], P('ep', 'tp')
- expert_output: bfloat16 [1024, 2048], P('ep', 'tp')
Inputs may be any that keep to these rules, and one draw needn't show every extreme that they name: `routes`: each row names 2 different experts. Among the 128 rows of one index of ep, no expert is named more than 64 times, a bound that some block reaches in some of them. `pole_real`: every rate is negative.
All inputs are finite; a program needn't handle non-finite values.
Results may differ from a plain program's by a relative error of at most 0.02.
Values may be sent and summed in bfloat16 or wider, within the bound.
A program may use at most 128 MiB of HBM per device.

v0:
```python
import functools
import jax
import jax.numpy as jnp
from jax import lax
from jax.experimental import pallas as pl
from jax.experimental.pallas import tpu as pltpu
from jax.sharding import PartitionSpec as P

norm_eps = 1e-05
highest = lax.Precision.HIGHEST
CHUNKS = 8
TILE = 256


def sin_cos(angle):
    turns = jnp.round(angle * 0.6366197723675814)
    left = angle - turns * 1.5703125
    left = left - turns * 4.83751296997e-4
    left = left - turns * 7.549789948768648e-8
    sq = left * left
    sine = ((-1.9515295891e-4 * sq + 8.3321608736e-3) * sq - 1.6666654611e-1) * sq * left + left
    cosine = (
        ((2.443315711809948e-5 * sq - 1.388731625493765e-3) * sq + 4.166664568298827e-2) * sq * sq
        - 0.5 * sq
        + 1.0
    )
    quadrant = turns.astype(jnp.int32)
    odd = (quadrant & 1) == 1
    sin_out = jnp.where(odd, cosine, sine)
    cos_out = jnp.where(odd, sine, cosine)
    sin_out = jnp.where((quadrant & 2) == 2, -sin_out, sin_out)
    cos_out = jnp.where(((quadrant + 1) & 2) == 2, -cos_out, cos_out)
    return sin_out, cos_out


def nt(left, right, **kw):
    return lax.dot_general(
        left, right, (((1,), (1,)), ((), ())), preferred_element_type=jnp.float32, **kw
    )


def spread(table, row_div, lane_div):
    rows, width = table.shape
    lanes = width * (rows // row_div)
    src = lax.broadcasted_iota(jnp.int32, (width, lanes), 0)
    dst = lax.broadcasted_iota(jnp.int32, (width, lanes), 1)
    pick = (src == dst % width).astype(jnp.bfloat16)
    wide = jnp.dot(table.astype(jnp.bfloat16), pick, preferred_element_type=jnp.float32)
    row = lax.broadcasted_iota(jnp.int32, (rows, lanes), 0) // row_div
    lane = lax.broadcasted_iota(jnp.int32, (rows, lanes), 1) // lane_div
    return jnp.where(row == lane, wide, 0.0).astype(jnp.bfloat16)


def mixer_kernel(
    width,
    rows_ref,
    stats_ref,
    gain_ref,
    step_ref,
    pole_ref,
    in_re_ref,
    in_im_ref,
    rd_re_ref,
    rd_im_ref,
    out_ref,
    a_re,
    a_im,
    u_re,
    u_im,
    sums,
    enter,
    mixed_ref,
    mine_ref,
    slots_ref,
    send_sems,
    recv_sems,
):
    count = slots_ref.shape[0]
    me = lax.axis_index("ep")
    barrier = pltpu.get_barrier_semaphore()
    for k in range(1, count):
        pl.semaphore_signal(
            barrier,
            inc=1,
            device_id={"ep": lax.rem(me + k, count)},
            device_id_type=pl.DeviceIdType.MESH,
        )

    positions, channels = rows_ref.shape
    groups = step_ref.shape[1]
    flat = a_re.shape[1]
    states = flat // groups
    group_ch = channels // groups
    tiles = flat // TILE
    per_tile = TILE // states
    tile_ch = per_tile * group_ch
    steps = positions // CHUNKS

    average = stats_ref[:, 0:1] / width
    variance = stats_ref[:, 1:2] / width - average * average
    normed = (rows_ref[...].astype(jnp.float32) - average) * lax.rsqrt(variance + norm_eps)
    normed = (normed * gain_ref[...]).astype(jnp.bfloat16)
    to_row = lax.broadcasted_iota(jnp.int32, (positions, positions), 0)
    from_row = lax.broadcasted_iota(jnp.int32, (positions, positions), 1)
    order = from_row == (to_row % CHUNKS) * steps + to_row // CHUNKS
    order16 = order.astype(jnp.bfloat16)
    normed = jnp.dot(order16, normed, preferred_element_type=jnp.float32).astype(jnp.bfloat16)
    step = jnp.dot(
        order.astype(jnp.float32), step_ref[...], precision=highest,
        preferred_element_type=jnp.float32,
    )

    for tile in range(tiles):
        lanes = slice(tile * TILE, (tile + 1) * TILE)
        source = lax.broadcasted_iota(jnp.int32, (groups, TILE), 0)
        owner = lax.broadcasted_iota(jnp.int32, (groups, TILE), 1) // states + tile * per_tile
        a_re[:, lanes] = jnp.dot(
            step, (source == owner).astype(jnp.float32), precision=highest,
            preferred_element_type=jnp.float32,
        )
        piece = normed[:, tile * tile_ch : (tile + 1) * tile_ch]
        u_re[:, lanes] = nt(piece, spread(in_re_ref[lanes, :], states, group_ch))
        u_im[:, lanes] = nt(piece, spread(in_im_ref[lanes, :], states, group_ch))
        p_re, p_im = pole_ref[0:1, lanes], pole_ref[1:2, lanes]
        d_re, d_im = pole_ref[2:3, lanes], pole_ref[3:4, lanes]

        def first(s, carried, lanes=lanes, p_re=p_re, p_im=p_im, d_re=d_re, d_im=d_im):
            c_re, c_im, s_re, s_im = carried
            here = pl.ds(pl.multiple_of(s * CHUNKS, CHUNKS), CHUNKS)
            delta = a_re[here, lanes]
            magnitude = jnp.exp(p_re * delta)
            sine, cosine = sin_cos(p_im * delta)
            ab_re = magnitude * cosine
            ab_im = magnitude * sine
            numer = ab_re - 1.0
            k_re = numer * d_re + ab_im * d_im
            k_im = ab_im * d_re - numer * d_im
            v_re, v_im = u_re[here, lanes], u_im[here, lanes]
            w_re = k_re * v_re - k_im * v_im
            w_im = k_re * v_im + k_im * v_re
            a_re[here, lanes] = ab_re
            a_im[here, lanes] = ab_im
            u_re[here, lanes] = w_re
            u_im[here, lanes] = w_im
            return (
                ab_re * c_re - ab_im * c_im,
                ab_re * c_im + ab_im * c_re,
                ab_re * s_re - ab_im * s_im + w_re,
                ab_re * s_im + ab_im * s_re + w_im,
            )

        zero = jnp.zeros((CHUNKS, TILE), jnp.float32)
        found = lax.fori_loop(0, steps, first, (zero + 1.0, zero, zero, zero), unroll=4)
        for index, part in enumerate(found):
            sums[index, :, lanes] = part

    def chunk(index, c):
        return sums[index, c : c + 1, :]

    c_re, c_im, s_re, s_im = (chunk(index, 0) for index in range(4))
    for c in range(1, CHUNKS):
        b_re, b_im = chunk(0, c), chunk(1, c)
        c_re, c_im = b_re * c_re - b_im * c_im, b_re * c_im + b_im * c_re
        s_re, s_im = (
            b_re * s_re - b_im * s_im + chunk(2, c),
            b_re * s_im + b_im * s_re + chunk(3, c),
        )
    mine_ref[0:1, :] = c_re
    mine_ref[1:2, :] = c_im
    mine_ref[2:3, :] = s_re
    mine_ref[3:4, :] = s_im

    pl.semaphore_wait(barrier, count - 1)
    copies = []
    for k in range(1, count):
        copy = pltpu.make_async_remote_copy(
            src_ref=mine_ref,
            dst_ref=slots_ref.at[k],
            send_sem=send_sems.at[k],
            recv_sem=recv_sems.at[k],
            device_id={"ep": lax.rem(me + k, count)},
            device_id_type=pl.DeviceIdType.MESH,
        )
        copy.start()
        copies.append(copy)
    read_re = [
        spread(rd_re_ref[t * tile_ch : (t + 1) * tile_ch, :], group_ch, states)
        for t in range(tiles)
    ]
    read_im = [
        spread(rd_im_ref[t * tile_ch : (t + 1) * tile_ch, :], group_ch, states)
        for t in range(tiles)
    ]
    for copy in copies:
        copy.wait()

    def fold(position, carried):
        h_re, h_im = carried
        slot = me - position
        b_re, b_im = slots_ref[slot, 0:1, :], slots_ref[slot, 1:2, :]
        return (
            b_re * h_re - b_im * h_im + slots_ref[slot, 2:3, :],
            b_re * h_im + b_im * h_re + slots_ref[slot, 3:4, :],
        )

    blank = jnp.zeros((1, flat), jnp.float32)
    h_re, h_im = lax.fori_loop(0, me, fold, (blank, blank))
    for c in range(CHUNKS):
        enter[0, c : c + 1, :] = h_re
        enter[1, c : c + 1, :] = h_im
        b_re, b_im = chunk(0, c), chunk(1, c)
        h_re, h_im = (
            b_re * h_re - b_im * h_im + chunk(2, c),
            b_re * h_im + b_im * h_re + chunk(3, c),
        )

    for tile in range(tiles):
        lanes = slice(tile * TILE, (tile + 1) * TILE)

        def second(s, carried, lanes=lanes):
            s_re, s_im = carried
            here = pl.ds(pl.multiple_of(s * CHUNKS, CHUNKS), CHUNKS)
            ab_re, ab_im = a_re[here, lanes], a_im[here, lanes]
            n_re = ab_re * s_re - ab_im * s_im + u_re[here, lanes]
            n_im = ab_re * s_im + ab_im * s_re + u_im[here, lanes]
            u_re[here, lanes] = n_re
            u_im[here, lanes] = n_im
            return n_re, n_im

        lax.fori_loop(0, steps, second, (enter[0, :, lanes], enter[1, :, lanes]), unroll=8)
        response = nt(u_re[:, lanes].astype(jnp.bfloat16), read_re[tile]) - nt(
            u_im[:, lanes].astype(jnp.bfloat16), read_im[tile]
        )
        mixed_ref[:, tile * tile_ch : (tile + 1) * tile_ch] = jax.nn.gelu(response).astype(
            jnp.bfloat16
        )
    back = (to_row == (from_row % CHUNKS) * steps + from_row // CHUNKS).astype(jnp.bfloat16)
    out_ref[...] = jnp.dot(
        back, mixed_ref[...], preferred_element_type=jnp.float32
    ).astype(jnp.bfloat16)


def mix(rows, stats, gain, step, pole, in_re, in_im, rd_re, rd_im, width):
    positions, channels = rows.shape
    flat = pole.shape[1]
    count = lax.axis_size("ep")
    f32 = jnp.float32
    return pl.pallas_call(
        functools.partial(mixer_kernel, width),
        out_shape=jax.ShapeDtypeStruct((positions, channels), jnp.bfloat16),
        in_specs=[pl.BlockSpec(memory_space=pltpu.VMEM)] * 9,
        out_specs=pl.BlockSpec(memory_space=pltpu.VMEM),
        scratch_shapes=[
            pltpu.VMEM((positions, flat), f32),
            pltpu.VMEM((positions, flat), f32),
            pltpu.VMEM((positions, flat), f32),
            pltpu.VMEM((positions, flat), f32),
            pltpu.VMEM((4, CHUNKS, flat), f32),
            pltpu.VMEM((2, CHUNKS, flat), f32),
            pltpu.VMEM((positions, channels), jnp.bfloat16),
            pltpu.VMEM((4, flat), f32),
            pltpu.VMEM((count, 4, flat), f32),
            pltpu.SemaphoreType.DMA((count,)),
            pltpu.SemaphoreType.DMA((count,)),
        ],
        compiler_params=pltpu.CompilerParams(
            collective_id=0, has_side_effects=True, vmem_limit_bytes=24 * 1024 * 1024
        ),
        cost_estimate=pl.CostEstimate(
            flops=2 * positions * flat * 400, bytes_accessed=4 * positions * flat, transcendentals=0
        ),
    )(rows, stats, gain, step, pole, in_re, in_im, rd_re, rd_im)


def row_moments(rows):
    wide = rows.astype(jnp.float32)
    return (jnp.sum(wide, axis=1), jnp.sum(wide * wide, axis=1))


def normalize(rows, sums, squares, gain, width):
    average = sums / width
    variance = squares / width - average * average
    wide = rows.astype(jnp.float32)
    return (wide - average[:, None]) * lax.rsqrt(variance[:, None] + norm_eps) * gain[None, :]


def shards(
    mixer_input,
    mixer_gain,
    time_step,
    pole_real,
    pole_imag,
    input_real,
    input_imag,
    read_real,
    read_imag,
    out_value,
    out_gate,
    expert_input,
    expert_gain,
    routes,
    route_weight,
    expert_gate,
    expert_up,
    expert_down,
):
    width = mixer_input.shape[1] * lax.axis_size("tp")
    sums_a, squares_a = row_moments(mixer_input)
    sums_b, squares_b = row_moments(expert_input)
    sums_a, squares_a, sums_b, squares_b = lax.psum((sums_a, squares_a, sums_b, squares_b), "tp")
    stats_a = jnp.stack([sums_a, squares_a], axis=1)
    normed_b = normalize(expert_input, sums_b, squares_b, expert_gain, width).astype(jnp.bfloat16)
    flat_real = pole_real.reshape(-1)
    flat_imag = pole_imag.reshape(-1)
    denom = flat_real * flat_real + flat_imag * flat_imag
    pole = jnp.stack([flat_real, flat_imag, flat_real / denom, flat_imag / denom])
    mixed = mix(
        mixer_input,
        stats_a,
        mixer_gain[None, :],
        time_step,
        pole,
        input_real.reshape(-1, input_real.shape[2]),
        input_imag.reshape(-1, input_imag.shape[2]),
        read_real.reshape(-1, read_real.shape[2]),
        read_imag.reshape(-1, read_imag.shape[2]),
        width,
    )
    piece = lax.all_gather(mixed, "tp", axis=1, tiled=True)
    value_sum = jnp.dot(piece, out_value, preferred_element_type=jnp.float32)
    gate_sum = jnp.dot(piece, out_gate, preferred_element_type=jnp.float32)
    mixer_output = (value_sum * jax.nn.sigmoid(gate_sum)).astype(jnp.bfloat16)
    tokens_dev, top_count = routes.shape
    expert_count = lax.axis_size("ep")
    capacity = 2 * top_count * tokens_dev // expert_count
    flat_routes = routes.reshape(-1)
    onehot = (flat_routes[:, None] == jnp.arange(expert_count, dtype=jnp.int32)[None, :]).astype(
        jnp.int32
    )
    earlier_hits = jnp.cumsum(onehot, axis=0) - onehot
    position = jnp.sum(earlier_hits * onehot, axis=1)
    slot_index = (flat_routes * capacity + position).reshape(tokens_dev, top_count)
    slots = jnp.arange(expert_count * capacity, dtype=jnp.int32)
    named = slot_index[:, :, None] == slots[None, None, :]
    gate_weight = expert_gate[0]
    up_weight = expert_up[0]
    down_weight = expert_down[0]
    full_rows = lax.all_gather(normed_b, "tp", axis=1, tiled=True)
    chosen = jnp.any(named, axis=1).astype(jnp.bfloat16)
    outgoing = lax.dot_general(
        chosen, full_rows, (((0,), (0,)), ((), ())), preferred_element_type=jnp.float32
    ).astype(jnp.bfloat16)
    arrived = lax.all_to_all(outgoing, "ep", split_axis=0, concat_axis=0, tiled=True)
    gate_val = jnp.dot(arrived, gate_weight, preferred_element_type=jnp.float32)
    up_val = jnp.dot(arrived, up_weight, preferred_element_type=jnp.float32)
    hidden = (jax.nn.silu(gate_val) * up_val).astype(jnp.bfloat16)
    summed = lax.psum_scatter(
        lax.dot_general(
            down_weight, hidden, (((0,), (1,)), ((), ())), preferred_element_type=jnp.float32
        ).astype(jnp.bfloat16),
        "tp",
        scatter_dimension=0,
        tiled=True,
    )
    returned = lax.all_to_all(summed, "ep", split_axis=1, concat_axis=1, tiled=True)
    share = jnp.sum(jnp.where(named, route_weight[:, :, None], 0.0), axis=1)
    share_high = share.astype(jnp.bfloat16)
    share_low = (share - share_high.astype(jnp.float32)).astype(jnp.bfloat16)
    expert_output = (nt(share_high, returned) + nt(share_low, returned)).astype(jnp.bfloat16)
    return (mixer_output, expert_output)


def solution(mesh):
    return jax.shard_map(
        shards,
        mesh=mesh,
        in_specs=(
            P("ep", "tp"),
            P("tp"),
            P("ep", "tp"),
            P("tp", None),
            P("tp", None),
            P("tp", None, None),
            P("tp", None, None),
            P("tp", None, None),
            P("tp", None, None),
            P(None, "tp"),
            P(None, "tp"),
            P("ep", "tp"),
            P("tp"),
            P("ep", None),
            P("ep", None),
            P("ep", None, "tp"),
            P("ep", None, "tp"),
            P("ep", "tp", None),
        ),
        out_specs=(P("ep", "tp"), P("ep", "tp")),
        check_vma=False,
    )
```

profile of v0, /device:TPU:0, one launch (start us, length us, event | category | flops | bytes accessed | tf_op | source)
XLA Modules:
  0.0 160.0 jit_solution(4754247642333787712)
XLA Ops:
  7.2 0.9 copy.57
  8.4 1.1 convert_reduce_fusion
  9.6 1.0 convert_reduce_fusion.1
  10.6 8.4 %all-reduce = (f32[256,1]{0,1:T(1,128)S(1)}, f32[256,1]{0,1:T(1,128)S(1)}, f32[128]{0:T(128)S(1)}, f32[128]{0:T(128)S(1)}) all-reduce(f32[256,1]{0,1:T(1,128)S(1)} %bitcast.60, f32[256,1]{0,1:T(1,128)S(1)} %bitcast.59, f32[128]{0:T(128)S(1)} %get-tuple-element.5, f32[128]{0:T(128)S(1)} %get-tuple-element.4), channel_id=1, replica_groups=mesh['ep'=8,'tp'=4] {'tp'}, use_global_device_ids=true, to_apply=%region_3.0 | all-reduce | flops 768 | bytes 6144 | tf_op jit(solution)/shard_map/psum | solution.py:310
  19.0 1.0 fusion.25
  20.0 6.5 %all_gather.7 = bf16[128,2048]{1,0:T(8,128)(2,1)S(1)} all-gather(bf16[128,512]{1,0:T(8,128)(2,1)S(1)} %fusion.25), channel_id=1, replica_groups=mesh['ep'=8,'tp'=4] {'tp'}, dimensions={1}, use_global_device_ids=true | all-gather | bytes 655360 | tf_op jit(solution)/shard_map/all_gather | solution.py:348
  28.5 0.8 convolution_convert_fusion
  29.3 54.6 %all_to_all.24 = bf16[8,64,2048]{2,1,0:T(8,128)(2,1)S(1)} all-to-all(bf16[8,64,2048]{2,1,0:T(8,128)(2,1)S(1)} %bitcast.53), channel_id=1, replica_groups=mesh['ep'=8,'tp'=4] {'ep'}, dimensions={0} | all-to-all | bytes 4194304 | tf_op jit(solution)/shard_map/all_to_all | solution.py:353
  83.8 1.3 copy-done.7
  85.2 3.6 %fusion.4 = f32[512,1024]{1,0:T(8,128)} fusion(bf16[512,2048]{1,0:T(8,128)(2,1)S(1)} %bitcast.56, bf16[1,2048,1024]{2,1,0:T(8,128)(2,1)S(1)} %copy-done.13), kind=kOutput, calls=%fused_computation.4 | convolution fusion | flops 2147483648 | bytes 8388608 | tf_op jit(solution)/shard_map/dot_general | solution.py:354
  88.8 10.6 %fusion.9 = bf16[2048,512]{0,1:T(8,128)(2,1)} fusion(bf16[1,1024,2048]{2,1,0:T(8,128)(2,1)} %param.35, f32[512,1024]{1,0:T(8,128)} %fusion.4, bf16[512,2048]{1,0:T(8,128)(2,1)} %bitcast.57, bf16[1,2048,1024]{2,1,0:T(8,128)(2,1)} %param.34), kind=kOutput, calls=%fused_computation.8 | convolution fusion | flops 4299161600 | bytes 14680064 | tf_op jit(solution)/shard_map/dot_general | solution.py:358
  100.6 1.2 copy.54
  101.8 1.5 copy.56.step_ref
  103.4 0.9 copy-done.3
  104.3 1.0 copy-done.4
  105.2 1.0 copy-done.5
  106.2 13.0 %shard_map.185 = bf16[256,512]{1,0:T(8,128)(2,1)S(1)} custom-call(bf16[256,512]{1,0:T(8,128)(2,1)S(1)} %copy-done.1, f32[256,2]{1,0:T(8,128)S(1)} %copy.55.stats_ref, f32[1,512]{1,0:T(1,128)S(1)} %bitcast.52, f32[256,32]{1,0:T(8,128)S(1)} %copy-done.3, f32[4,1024]{1,0:T(4,128)S(1)} %pad_maximum_fusion.pole_ref, f32[1024,16]{1,0:T(8,128)S(1)} %bitcast.48, ...), custom_call_target="tpu_custom_call" | custom-call | flops 209715200 | bytes 1048576 | tf_op jit(solution)/shard_map/pallas_call | solution.py:248
  120.0 9.6 %reduce-scatter.2.cloned.1.call-done = bf16[512,512]{0,1:T(8,128)(2,1)} async-done(((bf16[2048,512]{0,1:T(8,128)(2,1)}), bf16[512,512]{0,1:T(8,128)(2,1)}) %reduce-scatter.2.cloned.1.call-update) | async-done | bytes 524304 | tf_op jit(solution)/shard_map/reduce_scatter | solution.py:357
  129.5 5.5 %all-to-all-start.1 = ((bf16[512,8,64]{0,2,1:T(8,128)(2,1)}), bf16[512,8,64]{0,2,1:T(8,128)(2,1)S(1)}, u32[]{:S(2)}, u32[]{:S(2)}) async-start(bf16[512,8,64]{0,2,1:T(8,128)(2,1)} %bitcast.58), calls=%async_computation.2 | async-start | bytes 1048576 | tf_op jit(solution)/shard_map/all_to_all | solution.py:365
  135.0 0.8 select_reduce_fusion
  135.9 12.5 %all-gather.2.cloned.1.call-done = bf16[256,2048]{1,0:T(8,128)(2,1)} async-done(((bf16[256,512]{1,0:T(8,128)(2,1)}), bf16[256,2048]{1,0:T(8,128)(2,1)}) %all-gather.2.cloned.1.call-update) | async-done | bytes 1048592 | tf_op jit(solution)/shard_map/all_gather | solution.py:329
  148.4 2.2 %fusion.16 = f32[256,512]{1,0:T(8,128)S(1)} fusion(bf16[256,2048]{1,0:T(8,128)(2,1)} %all-gather.2.cloned.1.call-done, bf16[2048,512]{1,0:T(8,128)(2,1)S(1)} %copy-done), kind=kOutput, calls=%fused_computation.14 | convolution fusion | flops 537264128 | bytes 3670016 | tf_op jit(solution)/shard_map/dot_general | solution.py:331
  150.6 1.4 fusion.17
  152.2 0.9 fusion.18
  (50 shorter events, 4.4 us)
Async XLA Ops:
  7.2 141.2 %copy-start = (bf16[2048,512]{1,0:T(8,128)(2,1)S(1)}, bf16[2048,512]{1,0:T(8,128)(2,1)}, u32[]{:S(2)}) copy-start(bf16[2048,512]{1,0:T(8,128)(2,1)} %param.28) | copy-start | bytes 6291460
  7.2 122.3 %reduce-scatter.2.cloned.1.call-start = ((), (), s32[]{:S(2)}) async-start(), calls=%async_computation.4 | async-start | bytes 2621440 | tf_op jit(solution)/shard_map/reduce_scatter | solution.py:357
  29.2 55.9 %copy-start.13 = (bf16[1,2048,1024]{2,1,0:T(8,128)(2,1)S(1)}, bf16[1,2048,1024]{2,1,0:T(8,128)(2,1)}, u32[]{:S(2)}) copy-start(bf16[1,2048,1024]{2,1,0:T(8,128)(2,1)} %param.33) | copy-start | bytes 12582916
  83.8 1.3 copy-start.7
  99.4 0.7 copy-start.11
  99.4 0.8 copy-start.12
  99.4 1.0 copy-start.10
  99.4 3.9 %copy-start.1 = (bf16[256,512]{1,0:T(8,128)(2,1)S(1)}, bf16[256,512]{1,0:T(8,128)(2,1)}, u32[]{:S(2)}) copy-start(bf16[256,512]{1,0:T(8,128)(2,1)} %rows_ref.1) | copy-start | bytes 786436
  99.4 3.9 %copy-start.6 = (f32[512]{0:T(512)S(1)}, f32[512]{0:T(512)}, u32[]{:S(2)}) copy-start(f32[512]{0:T(512)} %param.19) | copy-start | bytes 6148
  99.4 48.9 %all-gather.2.cloned.1.call-start = ((), (), s32[]{:S(2)}) async-start(), calls=%async_computation.3 | async-start | bytes 1310720 | tf_op jit(solution)/shard_map/all_gather | solution.py:329
  103.4 0.9 copy-start.3
  104.3 1.0 copy-start.4
  105.2 1.0 copy-start.5
  119.2 0.7 copy-start.2
  129.5 22.5 %all-to-all-start.1 = ((bf16[512,8,64]{0,2,1:T(8,128)(2,1)}), bf16[512,8,64]{0,2,1:T(8,128)(2,1)S(1)}, u32[]{:S(2)}, u32[]{:S(2)}) async-start(bf16[512,8,64]{0,2,1:T(8,128)(2,1)} %bitcast.58), calls=%async_computation.2 | async-start | bytes 1048576 | tf_op jit(solution)/shard_map/all_to_all | solution.py:365
  148.4 2.2 %copy-start.8 = (bf16[2048,512]{1,0:T(8,128)(2,1)S(1)}, bf16[2048,512]{1,0:T(8,128)(2,1)}, u32[]{:S(2)}) copy-start(bf16[2048,512]{1,0:T(8,128)(2,1)} %param.27) | copy-start | bytes 6291460
  148.4 2.2 %copy-start.9 = (bf16[256,2048]{1,0:T(8,128)(2,1)S(1)}, bf16[256,2048]{1,0:T(8,128)(2,1)}, u32[]{:S(2)}) copy-start(bf16[256,2048]{1,0:T(8,128)(2,1)} %all-gather.2.cloned.1.call-done) | copy-start | bytes 3145732
Sparse Core Ops, SparseCore 0:
  99.6 29.9 reduce-scatter.1
  131.7 16.6 all-gather.1
where the time goes:
time: 161 us; the launch traced here: 160 us
  blocking collectives  69.5 us (43%)
  waiting for transfers between devices  22.1 us (14%)
  matrix products  19.7 us (12%)
  between operations  14.2 us (9%)
  Pallas kernels  13 us (8%)
  local copies, waits for them, and re-layouts  10.3 us (6%)
  starting transfers between devices  5.6 us (3%)
  other arithmetic  5.58 us (3%)
    all_to_all x1, blocking collectives, shards(): lax.all_to_all(outgoing, 'ep', split_axis=0, concat_axis=0, tiled=True)  54.6 us
    pallas_call x1, Pallas kernels, mix(): pl.pallas_call(functools.partial(mixer_kernel, width), out_shape=jax.Shap...  13 us
    all_gather x1, waiting for transfers between devices, shards(): piece = lax.all_gather(mixed, 'tp', axis=1, tiled=True)  12.5 us
    dot_general x1, matrix products, shards(): lax.dot_general(down_weight, hidden, (((0,), (1,)), ((), ())), preferred_...  10.6 us
    reduce_scatter x1, waiting for transfers between devices, shards(): lax.psum_scatter(lax.dot_general(down_weight, hidden, (((0,), (1,)), ((),...  9.57 us
    unnamed x32, local copies, waits for them, and re-layouts  9.3 us
    psum x1, blocking collectives, shards(): lax.psum((sums_a, squares_a, sums_b, squares_b), 'tp')  8.4 us
    all_gather x1, blocking collectives, shards(): full_rows = lax.all_gather(normed_b, 'tp', axis=1, tiled=True)  6.5 us
  transfers between devices with their start and end apart: 3, of which 2 were waited for; matrix products, arithmetic and copies ran while one was open for 5% of the time, Pallas kernels for 8%

commit v1 on v0

--- a/solution.py
+++ b/solution.py
@@ -272,9 +272,69 @@
     )(rows, stats, gain, step, pole, in_re, in_im, rd_re, rd_im)
 
 
-def row_moments(rows):
-    wide = rows.astype(jnp.float32)
-    return (jnp.sum(wide, axis=1), jnp.sum(wide * wide, axis=1))
+def moments_kernel(a_ref, b_ref, out_a_ref, out_b_ref, mine_ref, slots_ref, send_sems, recv_sems):
+    count = slots_ref.shape[0]
+    me = lax.axis_index("tp")
+    barrier = pltpu.get_barrier_semaphore()
+    for k in range(1, count):
+        pl.semaphore_signal(
+            barrier,
+            inc=1,
+            device_id={"tp": lax.rem(me + k, count)},
+            device_id_type=pl.DeviceIdType.MESH,
+        )
+    split = a_ref.shape[0]
+    ones = jnp.ones((8, a_ref.shape[1]), jnp.float32)
+    first = lax.broadcasted_iota(jnp.int32, (8, 1), 0) == 0
+    for rows_ref, lanes in ((a_ref, slice(0, split)), (b_ref, slice(split, None))):
+        wide = rows_ref[...].astype(jnp.float32)
+        sums = nt(ones, wide, precision=highest)
+        squares = nt(ones, wide * wide, precision=highest)
+        mine_ref[:, lanes] = jnp.where(first, sums, squares)
+    pl.semaphore_wait(barrier, count - 1)
+    copies = []
+    for k in range(1, count):
+        copy = pltpu.make_async_remote_copy(
+            src_ref=mine_ref,
+            dst_ref=slots_ref.at[k],
+            send_sem=send_sems.at[k],
+            recv_sem=recv_sems.at[k],
+            device_id={"tp": lax.rem(me + k, count)},
+            device_id_type=pl.DeviceIdType.MESH,
+        )
+        copy.start()
+        copies.append(copy)
+    total = mine_ref[...]
+    for k, copy in enumerate(copies):
+        copy.wait()
+        total = total + slots_ref[k + 1]
+    turned = total.T
+    out_a_ref[...] = turned[:split, :]
+    out_b_ref[...] = turned[split:, :]
+
+
+def moments(rows_a, rows_b):
+    count = lax.axis_size("tp")
+    size = rows_a.shape[0] + rows_b.shape[0]
+    f32 = jnp.float32
+    return pl.pallas_call(
+        moments_kernel,
+        out_shape=[
+            jax.ShapeDtypeStruct((rows_a.shape[0], 8), f32),
+            jax.ShapeDtypeStruct((rows_b.shape[0], 8), f32),
+        ],
+        in_specs=[pl.BlockSpec(memory_space=pltpu.VMEM)] * 2,
+        out_specs=[pl.BlockSpec(memory_space=pltpu.VMEM)] * 2,
+        scratch_shapes=[
+            pltpu.VMEM((8, size), f32),
+            pltpu.VMEM((count, 8, size), f32),
+            pltpu.SemaphoreType.DMA((count,)),
+            pltpu.SemaphoreType.DMA((count,)),
+        ],
+        compiler_params=pltpu.CompilerParams(
+            collective_id=1, has_side_effects=True, vmem_limit_bytes=16 * 1024 * 1024
+        ),
+    )(rows_a, rows_b)
 
 
 def normalize(rows, sums, squares, gain, width):
@@ -305,15 +365,35 @@
     expert_down,
 ):
     width = mixer_input.shape[1] * lax.axis_size("tp")
-    sums_a, squares_a = row_moments(mixer_input)
-    sums_b, squares_b = row_moments(expert_input)
-    sums_a, squares_a, sums_b, squares_b = lax.psum((sums_a, squares_a, sums_b, squares_b), "tp")
-    stats_a = jnp.stack([sums_a, squares_a], axis=1)
+    stats_a, stats_b = moments(mixer_input, expert_input)
+    sums_b, squares_b = stats_b[:, 0], stats_b[:, 1]
     normed_b = normalize(expert_input, sums_b, squares_b, expert_gain, width).astype(jnp.bfloat16)
+    tokens_dev, top_count = routes.shape
+    expert_count = lax.axis_size("ep")
+    capacity = 2 * top_count * tokens_dev // expert_count
+    flat_routes = routes.reshape(-1)
+    onehot = (flat_routes[:, None] == jnp.arange(expert_count, dtype=jnp.int32)[None, :]).astype(
+        jnp.int32
+    )
+    earlier_hits = jnp.cumsum(onehot, axis=0) - onehot
+    position = jnp.sum(earlier_hits * onehot, axis=1)
+    slot_index = (flat_routes * capacity + position).reshape(tokens_dev, top_count)
+    slots = jnp.arange(expert_count * capacity, dtype=jnp.int32)
+    named = slot_index[:, :, None] == slots[None, None, :]
+    gate_weight = expert_gate[0]
+    up_weight = expert_up[0]
+    down_weight = expert_down[0]
+    chosen = jnp.any(named, axis=1).astype(jnp.bfloat16)
+    outgoing = lax.dot_general(
+        chosen, normed_b, (((0,), (0,)), ((), ())), preferred_element_type=jnp.float32
+    ).astype(jnp.bfloat16)
+    arrived = lax.all_to_all(outgoing, "ep", split_axis=0, concat_axis=0, tiled=True)
     flat_real = pole_real.reshape(-1)
     flat_imag = pole_imag.reshape(-1)
     denom = flat_real * flat_real + flat_imag * flat_imag
     pole = jnp.stack([flat_real, flat_imag, flat_real / denom, flat_imag / denom])
+    arrived, stats_a = lax.optimization_barrier((arrived, stats_a))
+    arrived = lax.all_gather(arrived, "tp", axis=1, tiled=True)
     mixed = mix(
         mixer_input,
         stats_a,
@@ -326,31 +406,8 @@
         read_imag.reshape(-1, read_imag.shape[2]),
         width,
     )
+    arrived, mixed = lax.optimization_barrier((arrived, mixed))
     piece = lax.all_gather(mixed, "tp", axis=1, tiled=True)
-    value_sum = jnp.dot(piece, out_value, preferred_element_type=jnp.float32)
-    gate_sum = jnp.dot(piece, out_gate, preferred_element_type=jnp.float32)
-    mixer_output = (value_sum * jax.nn.sigmoid(gate_sum)).astype(jnp.bfloat16)
-    tokens_dev, top_count = routes.shape
-    expert_count = lax.axis_size("ep")
-    capacity = 2 * top_count * tokens_dev // expert_count
-    flat_routes = routes.reshape(-1)
-    onehot = (flat_routes[:, None] == jnp.arange(expert_count, dtype=jnp.int32)[None, :]).astype(
-        jnp.int32
-    )
-    earlier_hits = jnp.cumsum(onehot, axis=0) - onehot
-    position = jnp.sum(earlier_hits * onehot, axis=1)
-    slot_index = (flat_routes * capacity + position).reshape(tokens_dev, top_count)
-    slots = jnp.arange(expert_count * capacity, dtype=jnp.int32)
-    named = slot_index[:, :, None] == slots[None, None, :]
-    gate_weight = expert_gate[0]
-    up_weight = expert_up[0]
-    down_weight = expert_down[0]
-    full_rows = lax.all_gather(normed_b, "tp", axis=1, tiled=True)
-    chosen = jnp.any(named, axis=1).astype(jnp.bfloat16)
-    outgoing = lax.dot_general(
-        chosen, full_rows, (((0,), (0,)), ((), ())), preferred_element_type=jnp.float32
-    ).astype(jnp.bfloat16)
-    arrived = lax.all_to_all(outgoing, "ep", split_axis=0, concat_axis=0, tiled=True)
     gate_val = jnp.dot(arrived, gate_weight, preferred_element_type=jnp.float32)
     up_val = jnp.dot(arrived, up_weight, preferred_element_type=jnp.float32)
     hidden = (jax.nn.silu(gate_val) * up_val).astype(jnp.bfloat16)
@@ -362,6 +419,9 @@
         scatter_dimension=0,
         tiled=True,
     )
+    value_sum = jnp.dot(piece, out_value, preferred_element_type=jnp.float32)
+    gate_sum = jnp.dot(piece, out_gate, preferred_element_type=jnp.float32)
+    mixer_output = (value_sum * jax.nn.sigmoid(gate_sum)).astype(jnp.bfloat16)
     returned = lax.all_to_all(summed, "ep", split_axis=1, concat_axis=1, tiled=True)
     share = jnp.sum(jnp.where(named, route_weight[:, :, None], 0.0), axis=1)
     share_high = share.astype(jnp.bfloat16)

time: 161 us -> 140 us (0.87)
  blocking collectives: 69.5 us -> 20.5 us
  waiting for transfers between devices: 22.1 us -> 46.8 us
  Pallas kernels: 13 us -> 19.7 us
  other arithmetic: 5.58 us -> 1.89 us
  matrix products: 19.7 us -> 22.8 us
  local copies, waits for them, and re-layouts: 10.3 us -> 8 us
    all_to_all x1, blocking collectives: 54.6 us -> 20.5 us  [shards(): lax.all_to_all(outgoing, 'ep', split_axis=0, concat_axis=0, tiled=True)]
    reduce_scatter x1, waiting for transfers between devices: 9.57 us -> 30.6 us  [shards(): lax.psum_scatter(lax.dot_general(down_weight, hidden, (((0,), (1,)), ((),...]
    psum x1 -> x0, blocking collectives: 8.4 us -> none  [shards(): lax.psum((sums_a, squares_a, sums_b, squares_b), 'tp')]
    all_gather x1 -> x0, blocking collectives: 6.5 us -> none  [shards(): full_rows = lax.all_gather(normed_b, 'tp', axis=1, tiled=True)]
    pallas_call x0 -> x1, Pallas kernels: none -> 6.22 us  [moments(): pl.pallas_call(moments_kernel, out_shape=[jax.ShapeDtypeStruct((rows_a.sh...]
    all_gather x0 -> x1, waiting for transfers between devices: none -> 2.85 us  [shards(): arrived = lax.all_gather(arrived, 'tp', axis=1, tiled=True)]
    dot_general x1, matrix products: 3.65 us -> 6.46 us  [shards(): gate_val = jnp.dot(arrived, gate_weight, preferred_element_type=jnp.float32)]
    unnamed x32 -> x36, local copies, waits for them, and re-layouts: 9.3 us -> 7.14 us
  transfers between devices with their start and end apart: 3 -> 4, of which waited for: 2 -> 3; matrix products, arithmetic and copies ran while one was open for 5% -> 4% of each run, Pallas kernels for 8% -> 10%
where the time goes in v1:
time: 140 us; the launch traced here: 139 us
  waiting for transfers between devices  46.8 us (33%)
  matrix products  22.8 us (16%)
  blocking collectives  20.5 us (15%)
  Pallas kernels  19.7 us (14%)
  between operations  14 us (10%)
  local copies, waits for them, and re-layouts  8 us (6%)
  starting transfers between devices  5.63 us (4%)
  other arithmetic  1.89 us (1%)
    reduce_scatter x1, waiting for transfers between devices, shards(): lax.psum_scatter(lax.dot_general(down_weight, hidden, (((0,), (1,)), ((),...  30.6 us
    all_to_all x1, blocking collectives, shards(): lax.all_to_all(outgoing, 'ep', split_axis=0, concat_axis=0, tiled=True)  20.5 us
    pallas_call x1, Pallas kernels, mix(): pl.pallas_call(functools.partial(mixer_kernel, width), out_shape=jax.Shap...  13.5 us
    all_gather x1, waiting for transfers between devices, shards(): piece = lax.all_gather(mixed, 'tp', axis=1, tiled=True)  12.6 us
    dot_general x1, matrix products, shards(): lax.dot_general(down_weight, hidden, (((0,), (1,)), ((), ())), preferred_...  10.5 us
    unnamed x36, local copies, waits for them, and re-layouts  7.14 us
    dot_general x1, matrix products, shards(): gate_val = jnp.dot(arrived, gate_weight, preferred_element_type=jnp.float32)  6.46 us
    pallas_call x1, Pallas kernels, moments(): pl.pallas_call(moments_kernel, out_shape=[jax.ShapeDtypeStruct((rows_a.sh...  6.22 us
  transfers between devices with their start and end apart: 4, of which 3 were waited for; matrix products, arithmetic and copies ran while one was open for 4% of the time, Pallas kernels for 10%

profile of v1, /device:TPU:0, one launch (start us, length us, event | category | flops | bytes accessed | tf_op | source)
XLA Modules:
  0.0 139.3 jit_solution(16979764318124036610)
XLA Ops:
  7.3 0.9 copy.41
  8.5 0.6 reduce-window.6
  9.6 0.7 multiply_add_fusion.1
  10.5 0.9 copy-done.1
  11.4 0.9 copy-done.3
  12.3 6.2 %shard_map.185 = (f32[256,8]{1,0:T(8,128)S(1)}, f32[128,8]{1,0:T(8,128)S(1)}) custom-call(bf16[256,512]{1,0:T(8,128)(2,1)S(1)} %copy-done.1, bf16[128,512]{1,0:T(8,128)(2,1)S(1)} %copy-done.3), custom_call_target="tpu_custom_call" | custom-call | tf_op jit(solution)/shard_map/pallas_call | solution.py:320
  18.8 1.1 convolution_convert_fusion
  19.9 20.5 %all_to_all.24 = bf16[8,64,512]{2,1,0:T(8,128)(2,1)} all-to-all(bf16[8,64,512]{2,1,0:T(8,128)(2,1)S(1)} %bitcast.53), channel_id=1, replica_groups=mesh['ep'=8,'tp'=4] {'ep'}, dimensions={0} | all-to-all | bytes 1048576 | tf_op jit(solution)/shard_map/all_to_all | solution.py:390
  41.0 1.2 copy.45
  42.2 0.9 copy-done.4
  43.2 0.9 copy-done.5
  44.1 0.9 copy-done.7
  45.0 13.5 %shard_map.186 = bf16[256,512]{1,0:T(8,128)(2,1)} custom-call(bf16[256,512]{1,0:T(8,128)(2,1)S(1)} %copy-done.2, f32[256,8]{1,0:T(8,128)S(1)} %copy-done.7, f32[1,512]{1,0:T(1,128)S(1)} %bitcast.49, f32[256,32]{1,0:T(8,128)S(1)} %copy.46.step_ref, f32[4,1024]{1,0:T(4,128)S(1)} %pad_maximum_fusion.pole_ref, f32[1024,16]{1,0:T(8,128)S(1)} %bitcast.45, ...), custom_call_target="tpu_custom_call" | custom-call | flops 209715200 | bytes 1048576 | tf_op jit(solution)/shard_map/pallas_call | solution.py:248
  58.5 2.8 %all-gather.3.cloned.1.call-done = bf16[512,2048]{1,0:T(8,128)(2,1)} async-done(((bf16[512,512]{1,0:T(8,128)(2,1)}), bf16[512,2048]{1,0:T(8,128)(2,1)}) %all-gather.3.cloned.1.call-update) | async-done | bytes 2097168 | tf_op jit(solution)/shard_map/all_gather | solution.py:396
  61.4 6.5 %fusion.4 = f32[512,1024]{1,0:T(8,128)} fusion(bf16[512,2048]{1,0:T(8,128)(2,1)} %all-gather.3.cloned.1.call-done, bf16[1,2048,1024]{2,1,0:T(8,128)(2,1)} %param.33), kind=kOutput, calls=%fused_computation.4 | convolution fusion | flops 2147483648 | bytes 8388608 | tf_op jit(solution)/shard_map/dot_general | solution.py:411
  67.8 10.5 %fusion.9 = bf16[2048,512]{0,1:T(8,128)(2,1)} fusion(bf16[1,1024,2048]{2,1,0:T(8,128)(2,1)} %param.35, f32[512,1024]{1,0:T(8,128)} %fusion.4, bf16[512,2048]{1,0:T(8,128)(2,1)} %all-gather.3.cloned.1.call-done, bf16[1,2048,1024]{2,1,0:T(8,128)(2,1)} %param.34), kind=kOutput, calls=%fused_computation.7 | convolution fusion | flops 4299161600 | bytes 14680064 | tf_op jit(solution)/shard_map/dot_general | solution.py:415
  78.5 0.7 all-gather.5.cloned.1.call-update
  79.1 30.6 %reduce-scatter.2.cloned.1.call-done = bf16[512,512]{0,1:T(8,128)(2,1)} async-done(((bf16[2048,512]{0,1:T(8,128)(2,1)}), bf16[512,512]{0,1:T(8,128)(2,1)}) %reduce-scatter.2.cloned.1.call-update) | async-done | bytes 524304 | tf_op jit(solution)/shard_map/reduce_scatter | solution.py:414
  109.7 5.5 %all-to-all-start.1 = ((bf16[512,8,64]{0,2,1:T(8,128)(2,1)}), bf16[512,8,64]{0,2,1:T(8,128)(2,1)S(1)}, u32[]{:S(2)}, u32[]{:S(2)}) async-start(bf16[512,8,64]{0,2,1:T(8,128)(2,1)} %bitcast.54), calls=%async_computation.2 | async-start | bytes 1048576 | tf_op jit(solution)/shard_map/all_to_all | solution.py:425
  115.4 12.6 %all-gather.5.cloned.1.call-done = bf16[256,2048]{1,0:T(8,128)(2,1)} async-done(((bf16[256,512]{1,0:T(8,128)(2,1)}), bf16[256,2048]{1,0:T(8,128)(2,1)}) %all-gather.5.cloned.1.call-update) | async-done | bytes 1048592 | tf_op jit(solution)/shard_map/all_gather | solution.py:410
  128.1 2.2 %fusion.16 = f32[256,512]{1,0:T(8,128)S(1)} fusion(bf16[256,2048]{1,0:T(8,128)(2,1)} %all-gather.5.cloned.1.call-done, bf16[2048,512]{1,0:T(8,128)(2,1)S(1)} %copy-done), kind=kOutput, calls=%fused_computation.14 | convolution fusion | flops 537264128 | bytes 3670016 | tf_op jit(solution)/shard_map/dot_general | solution.py:423
  130.2 1.4 %fusion.17 = bf16[256,512]{1,0:T(8,128)(2,1)} fusion(f32[256,512]{1,0:T(8,128)S(1)} %fusion.16, bf16[256,2048]{1,0:T(8,128)(2,1)S(1)} %copy-done.10, bf16[2048,512]{1,0:T(8,128)(2,1)S(1)} %copy-done.9), kind=kOutput, calls=%fused_computation.15 | convolution fusion | flops 537133056 | bytes 3932160 | tf_op jit(solution)/shard_map/dot_general | solution.py:422
  131.7 0.2 fusion.26
  131.9 0.9 fusion.18
  (51 shorter events, 2.0 us)
Async XLA Ops:
  7.2 120.9 %copy-start = (bf16[2048,512]{1,0:T(8,128)(2,1)S(1)}, bf16[2048,512]{1,0:T(8,128)(2,1)}, u32[]{:S(2)}) copy-start(bf16[2048,512]{1,0:T(8,128)(2,1)} %param.28) | copy-start | bytes 6291460
  7.2 33.3 %copy-start.12 = (f32[256,32]{0,1:T(8,128)S(1)}, f32[256,32]{0,1:T(8,128)}, u32[]{:S(2)}) copy-start(f32[256,32]{0,1:T(8,128)} %param.20) | copy-start | bytes 98308
  7.2 33.4 %copy-start.13 = (f32[32,32]{1,0:T(8,128)S(1)}, f32[32,32]{1,0:T(8,128)}, u32[]{:S(2)}) copy-start(f32[32,32]{1,0:T(8,128)} %param.21) | copy-start | bytes 12292
  7.2 33.5 %copy-start.14 = (f32[32,32]{1,0:T(8,128)S(1)}, f32[32,32]{1,0:T(8,128)}, u32[]{:S(2)}) copy-start(f32[32,32]{1,0:T(8,128)} %param.22) | copy-start | bytes 12292
  7.2 33.5 %copy-start.11 = (f32[32,32,16]{1,2,0:T(8,128)S(1)}, f32[32,32,16]{1,2,0:T(8,128)}, u32[]{:S(2)}) copy-start(f32[32,32,16]{1,2,0:T(8,128)} %param.23) | copy-start | bytes 196612
  7.2 54.2 %all-gather.3.cloned.1.call-start = ((), (), s32[]{:S(2)}) async-start(), calls=%async_computation.3 | async-start | bytes 2621440 | tf_op jit(solution)/shard_map/all_gather | solution.py:396
  10.5 1.0 copy-start.1
  11.4 0.9 copy-start.3
  18.6 1.4 copy-start.6
  18.7 23.4 %copy-start.2 = (bf16[256,512]{1,0:T(8,128)(2,1)S(1)}, bf16[256,512]{1,0:T(8,128)(2,1)}, u32[]{:S(2)}) copy-start(bf16[256,512]{1,0:T(8,128)(2,1)} %rows_ref.1) | copy-start | bytes 786436
  18.8 23.4 %copy-start.8 = (f32[512]{0:T(512)S(1)}, f32[512]{0:T(512)}, u32[]{:S(2)}) copy-start(f32[512]{0:T(512)} %param.19) | copy-start | bytes 6148
  40.4 69.3 %reduce-scatter.2.cloned.1.call-start = ((), (), s32[]{:S(2)}) async-start(), calls=%async_computation.5 | async-start | bytes 2621440 | tf_op jit(solution)/shard_map/reduce_scatter | solution.py:414
  42.2 1.0 copy-start.4
  43.2 0.9 copy-start.5
  44.1 0.9 copy-start.7
  78.4 36.9 %copy-start.15 = (f32[128,2]{0,1:T(2,128)S(1)}, f32[128,2]{0,1:T(2,128)}, u32[]{:S(2)}) copy-start(f32[128,2]{0,1:T(2,128)} %param.32) | copy-start | bytes 3076
  78.4 49.6 %all-gather.5.cloned.1.call-start = ((), (), s32[]{:S(2)}) async-start(), calls=%async_computation.4 | async-start | bytes 1310720 | tf_op jit(solution)/shard_map/all_gather | solution.py:410
  109.7 21.9 %all-to-all-start.1 = ((bf16[512,8,64]{0,2,1:T(8,128)(2,1)}), bf16[512,8,64]{0,2,1:T(8,128)(2,1)S(1)}, u32[]{:S(2)}, u32[]{:S(2)}) async-start(bf16[512,8,64]{0,2,1:T(8,128)(2,1)} %bitcast.54), calls=%async_computation.2 | async-start | bytes 1048576 | tf_op jit(solution)/shard_map/all_to_all | solution.py:425
  128.0 2.2 %copy-start.9 = (bf16[2048,512]{1,0:T(8,128)(2,1)S(1)}, bf16[2048,512]{1,0:T(8,128)(2,1)}, u32[]{:S(2)}) copy-start(bf16[2048,512]{1,0:T(8,128)(2,1)} %param.27) | copy-start | bytes 6291460
  128.1 2.2 %copy-start.10 = (bf16[256,2048]{1,0:T(8,128)(2,1)S(1)}, bf16[256,2048]{1,0:T(8,128)(2,1)}, u32[]{:S(2)}) copy-start(bf16[256,2048]{1,0:T(8,128)(2,1)} %all-gather.5.cloned.1.call-done) | copy-start | bytes 3145732
Sparse Core Ops, SparseCore 0:
  40.5 20.7 all-gather.2
  78.5 31.1 reduce-scatter.1
  111.3 16.6 all-gather.4

commit v2 on v1

--- a/solution.py
+++ b/solution.py
@@ -344,6 +344,27 @@
     return (wide - average[:, None]) * lax.rsqrt(variance[:, None] + norm_eps) * gain[None, :]
 
 
+def scatter_sum(partial):
+    count = lax.axis_size("tp")
+    if count != 4:
+        return lax.psum_scatter(partial, "tp", scatter_dimension=0, tiled=True)
+    blocks = partial.reshape(count, partial.shape[0] // count, partial.shape[1])
+    me = lax.axis_index("tp")
+    core, far = me % 2, 2 - me // 2 * 2
+
+    def block(index):
+        return lax.dynamic_index_in_dim(blocks, index, 0, keepdims=False)
+
+    cores = [(0, 1), (1, 0), (2, 3), (3, 2)]
+    chips = [(0, 2), (2, 0), (1, 3), (3, 1)]
+    got_far = lax.ppermute(block(far + 1 - core), "tp", cores)
+    got_near = lax.ppermute(block(2 - far + 1 - core), "tp", cores)
+    half = block(far + core).astype(jnp.float32) + got_far.astype(jnp.float32)
+    across = lax.ppermute(half.astype(jnp.bfloat16), "tp", chips)
+    near = block(me).astype(jnp.float32) + got_near.astype(jnp.float32)
+    return (near + across.astype(jnp.float32)).astype(jnp.bfloat16)
+
+
 def shards(
     mixer_input,
     mixer_gain,
@@ -411,14 +432,11 @@
     gate_val = jnp.dot(arrived, gate_weight, preferred_element_type=jnp.float32)
     up_val = jnp.dot(arrived, up_weight, preferred_element_type=jnp.float32)
     hidden = (jax.nn.silu(gate_val) * up_val).astype(jnp.bfloat16)
-    summed = lax.psum_scatter(
-        lax.dot_general(
-            down_weight, hidden, (((0,), (1,)), ((), ())), preferred_element_type=jnp.float32
-        ).astype(jnp.bfloat16),
-        "tp",
-        scatter_dimension=0,
-        tiled=True,
-    )
+    hidden, piece = lax.optimization_barrier((hidden, piece))
+    partial = lax.dot_general(
+        down_weight, hidden, (((0,), (1,)), ((), ())), preferred_element_type=jnp.float32
+    ).astype(jnp.bfloat16)
+    summed = scatter_sum(partial)
     value_sum = jnp.dot(piece, out_value, preferred_element_type=jnp.float32)
     gate_sum = jnp.dot(piece, out_gate, preferred_element_type=jnp.float32)
     mixer_output = (value_sum * jax.nn.sigmoid(gate_sum)).astype(jnp.bfloat16)

time: 140 us -> 141 us (level)
  local copies, waits for them, and re-layouts: 8 us -> 15.9 us
  waiting for transfers between devices: 46.8 us -> 39.6 us
  other arithmetic: 1.89 us -> 5.28 us
  matrix products: 22.8 us -> 19.5 us
    reduce_scatter x1 -> x0, waiting for transfers between devices: 30.6 us -> none  [shards(): lax.psum_scatter(lax.dot_general(down_weight, hidden, (((0,), (1,)), ((),...]
    ppermute x0 -> x3, waiting for transfers between devices: none -> 15.6 us  [the longest x1 14 us: scatter_sum(): across = lax.ppermute(half.astype(jnp.bfloat16), 'tp', chips)]
    all_to_all x1, waiting for transfers between devices: 0.01 us -> 10.3 us  [shards(): lax.all_to_all(summed, 'ep', split_axis=1, concat_axis=1, tiled=True)]
    dot_general x1, matrix products: 10.5 us -> 5.85 us  [shards(): lax.dot_general(down_weight, hidden, (((0,), (1,)), ((), ())), preferred_...]
    reshape x0 -> x1, local copies, waits for them, and re-layouts: none -> 3.92 us  [scatter_sum(): blocks = partial.reshape(count, partial.shape[0] // count, partial.shape[1])]
    convert_element_type x0 -> x2, other arithmetic: none -> 3.38 us  [the longest x1 1.98 us: scatter_sum(): across = lax.ppermute(half.astype(jnp.bfloat16), 'tp', chips)]
    dot_general x0 -> x1, matrix products: none -> 2.51 us  [shards(): up_val = jnp.dot(arrived, up_weight, preferred_element_type=jnp.float32)]
    squeeze x0 -> x1, local copies, waits for them, and re-layouts: none -> 2.26 us  [block(): return lax.dynamic_index_in_dim(blocks, index, 0, keepdims=False)]
  transfers between devices with their start and end apart: 4 -> 6, of which waited for: 3 -> 5; matrix products, arithmetic and copies ran while one was open for 4% -> 11% of each run, Pallas kernels for 10% -> 9%
where the time goes in v2:
time: 141 us
  waiting for transfers between devices  39.6 us (28%)
  blocking collectives  20.5 us (15%)
  matrix products  19.5 us (14%)
  Pallas kernels  19.2 us (14%)
  local copies, waits for them, and re-layouts  15.9 us (11%)
  between operations  14.4 us (10%)
  starting transfers between devices  6.45 us (5%)
  other arithmetic  5.28 us (4%)
    all_to_all x1, blocking collectives, shards(): lax.all_to_all(outgoing, 'ep', split_axis=0, concat_axis=0, tiled=True)  20.5 us
    ppermute x1, waiting for transfers between devices, scatter_sum(): across = lax.ppermute(half.astype(jnp.bfloat16), 'tp', chips)  14 us
    pallas_call x1, Pallas kernels, mix(): pl.pallas_call(functools.partial(mixer_kernel, width), out_shape=jax.Shap...  13 us
    all_gather x1, waiting for transfers between devices, shards(): piece = lax.all_gather(mixed, 'tp', axis=1, tiled=True)  10.9 us
    all_to_all x1, waiting for transfers between devices, shards(): lax.all_to_all(summed, 'ep', split_axis=1, concat_axis=1, tiled=True)  10.3 us
    unnamed x42, local copies, waits for them, and re-layouts  7.86 us
    pallas_call x1, Pallas kernels, moments(): pl.pallas_call(moments_kernel, out_shape=[jax.ShapeDtypeStruct((rows_a.sh...  6.22 us
    dot_general x1, matrix products, shards(): lax.dot_general(down_weight, hidden, (((0,), (1,)), ((), ())), preferred_...  5.85 us
  transfers between devices with their start and end apart: 6, of which 5 were waited for; matrix products, arithmetic and copies ran while one was open for 11% of the time, Pallas kernels for 9%

profile of v2, /device:TPU:0, one launch (start us, length us, event | category | flops | bytes accessed | tf_op | source)
XLA Modules:
  0.0 140.7 jit_solution(13552003196717262402)
XLA Ops:
  10.5 0.9 copy-done.1
  12.3 6.2 %shard_map.185 = (f32[256,8]{1,0:T(8,128)S(1)}, f32[128,8]{1,0:T(8,128)S(1)}) custom-call(bf16[256,512]{1,0:T(8,128)(2,1)S(1)} %copy-done.1, bf16[128,512]{1,0:T(8,128)(2,1)S(1)} %copy-done.4), custom_call_target="tpu_custom_call" | custom-call | tf_op jit(solution)/shard_map/pallas_call | solution.py:320
  18.8 1.1 convolution_convert_fusion
  19.9 20.5 %all_to_all.24 = bf16[8,64,512]{2,1,0:T(8,128)(2,1)} all-to-all(bf16[8,64,512]{2,1,0:T(8,128)(2,1)S(1)} %bitcast.66), channel_id=1, replica_groups=mesh['ep'=8,'tp'=4] {'ep'}, dimensions={0} | all-to-all | bytes 1048576 | tf_op jit(solution)/shard_map/all_to_all | solution.py:411
  41.0 1.2 copy.68
  42.2 0.9 copy-done.5
  43.2 0.9 copy-done.6
  45.0 13.0 %shard_map.186 = bf16[256,512]{1,0:T(8,128)(2,1)S(1)} custom-call(bf16[256,512]{1,0:T(8,128)(2,1)S(1)} %copy-done.2, f32[256,8]{1,0:T(8,128)S(1)} %copy-done.8, f32[1,512]{1,0:T(1,128)S(1)} %bitcast.59, f32[256,32]{1,0:T(8,128)S(1)} %copy.69.step_ref, f32[4,1024]{1,0:T(4,128)S(1)} %pad_maximum_fusion.pole_ref, f32[1024,16]{1,0:T(8,128)S(1)} %bitcast.55, ...), custom_call_target="tpu_custom_call" | custom-call | flops 209715200 | bytes 1048576 | tf_op jit(solution)/shard_map/pallas_call | solution.py:248
  58.7 2.7 %all-gather.3.cloned.1.call-done = bf16[512,2048]{1,0:T(8,128)(2,1)} async-done(((bf16[512,512]{1,0:T(8,128)(2,1)}), bf16[512,2048]{1,0:T(8,128)(2,1)}) %all-gather.3.cloned.1.call-update) | async-done | bytes 2097168 | tf_op jit(solution)/shard_map/all_gather | solution.py:417
  61.5 5.3 %fusion.4 = f32[512,1024]{1,0:T(8,128)S(1)} fusion(bf16[512,2048]{1,0:T(8,128)(2,1)} %all-gather.3.cloned.1.call-done, bf16[1,2048,1024]{2,1,0:T(8,128)(2,1)} %param.33), kind=kOutput, calls=%fused_computation.4 | convolution fusion | flops 2147483648 | bytes 8388608 | tf_op jit(solution)/shard_map/dot_general | solution.py:432
  66.8 2.5 %multiply_convert_fusion = bf16[512,1024]{1,0:T(8,128)(2,1)S(1)} fusion(f32[512,1024]{1,0:T(8,128)S(1)} %fusion.4, bf16[512,2048]{1,0:T(8,128)(2,1)S(1)} %copy-done.18, bf16[1,2048,1024]{2,1,0:T(8,128)(2,1)S(1)} %copy-done.17), kind=kOutput, calls=%fused_computation.8 | convolution fusion | flops 2150629376 | bytes 9437184 | tf_op jit(solution)/shard_map/dot_general | solution.py:433
  69.3 10.9 %all-gather.5.cloned.1.call-done = bf16[256,2048]{1,0:T(8,128)(2,1)} async-done(((bf16[256,512]{1,0:T(8,128)(2,1)}), bf16[256,2048]{1,0:T(8,128)(2,1)}) %all-gather.5.cloned.1.call-update) | async-done | bytes 1048592 | tf_op jit(solution)/shard_map/all_gather | solution.py:431
  80.2 5.8 %fusion.9 = bf16[2048,512]{0,1:T(8,128)(2,1)} fusion(bf16[512,1024]{1,0:T(8,128)(2,1)S(1)} %multiply_convert_fusion, bf16[1,1024,2048]{2,1,0:T(8,128)(2,1)} %param.35), kind=kOutput, calls=%fused_computation.7 | convolution fusion | flops 2148532224 | bytes 7340032 | tf_op jit(solution)/shard_map/dot_general | solution.py:436
  86.1 3.9 %copy.75 = bf16[2048,512]{1,0:T(8,128)(2,1)} copy(bf16[2048,512]{0,1:T(8,128)(2,1)} %fusion.9) | data formatting | bytes 4194304 | tf_op jit(solution)/shard_map/reshape | solution.py:351
  90.0 2.3 %dynamic-slice_bitcast_fusion.1 = (bf16[512,512]{1,0:T(8,128)(2,1)}, bf16[512,512]{1,0:T(8,128)(2,1)}) fusion(bf16[4,512,512]{2,1,0:T(8,128)(2,1)} %bitcast.60, s32[]{:T(128)S(6)} %select_n.32, s32[]{:T(128)S(6)} %select_n.34), kind=kLoop, calls=%fused_computation.24 | loop fusion | bytes 2097160 | tf_op jit(solution)/shard_map/jit(dynamic_index_in_dim)/squeeze | solution.py:356
  92.8 1.6 %collective-permute-done.1 = bf16[512,512]{1,0:T(8,128)(2,1)S(1)} collective-permute-done((bf16[512,512]{1,0:T(8,128)(2,1)}, bf16[512,512]{1,0:T(8,128)(2,1)S(1)}, u32[]{:S(2)}, u32[]{:S(2)}) %collective-permute-start.1) | collective-permute-done | bytes 524320 | tf_op jit(solution)/shard_map/ppermute | solution.py:360
  94.4 2.0 %fusion.19 = bf16[512,512]{1,0:T(8,128)(2,1)} fusion(bf16[512,512]{1,0:T(8,128)(2,1)S(1)} %collective-permute-done.1, bf16[4,512,512]{2,1,0:T(8,128)(2,1)} %bitcast.61, s32[]{:T(128)S(6)} %select_n.33), kind=kLoop, calls=%fused_computation.19 | loop fusion | flops 1048576 | bytes 1572868 | tf_op jit(solution)/shard_map/convert_element_type | solution.py:363
  96.7 14.0 %collective-permute-done.2 = bf16[512,512]{1,0:T(8,128)(2,1)} collective-permute-done((bf16[512,512]{1,0:T(8,128)(2,1)}, bf16[512,512]{1,0:T(8,128)(2,1)}, u32[]{:S(2)}, u32[]{:S(2)}) %collective-permute-start.2) | collective-permute-done | bytes 524320 | tf_op jit(solution)/shard_map/ppermute | solution.py:363
  110.7 1.4 fusion.21
  112.1 1.0 copy.74
  113.2 5.5 %all-to-all-start.1 = ((bf16[512,8,64]{0,2,1:T(8,128)(2,1)}), bf16[512,8,64]{0,2,1:T(8,128)(2,1)S(1)}, u32[]{:S(2)}, u32[]{:S(2)}) async-start(bf16[512,8,64]{0,2,1:T(8,128)(2,1)} %bitcast.17), calls=%async_computation.1 | async-start | bytes 1048576 | tf_op jit(solution)/shard_map/all_to_all | solution.py:443
  118.8 2.2 %fusion.16 = f32[256,512]{1,0:T(8,128)S(1)} fusion(bf16[256,2048]{1,0:T(8,128)(2,1)} %all-gather.5.cloned.1.call-done, bf16[2048,512]{1,0:T(8,128)(2,1)S(1)} %copy-done), kind=kOutput, calls=%fused_computation.14 | convolution fusion | flops 537264128 | bytes 3670016 | tf_op jit(solution)/shard_map/dot_general | solution.py:441
  121.0 1.4 %fusion.17 = bf16[256,512]{1,0:T(8,128)(2,1)} fusion(f32[256,512]{1,0:T(8,128)S(1)} %fusion.16, bf16[256,2048]{1,0:T(8,128)(2,1)S(1)} %copy-done.11, bf16[2048,512]{1,0:T(8,128)(2,1)S(1)} %copy-done.10), kind=kOutput, calls=%fused_computation.15 | convolution fusion | flops 537133056 | bytes 3932160 | tf_op jit(solution)/shard_map/dot_general | solution.py:440
  122.4 10.3 %all-to-all-done.1 = bf16[512,8,64]{0,2,1:T(8,128)(2,1)S(1)} async-done(((bf16[512,8,64]{0,2,1:T(8,128)(2,1)}), bf16[512,8,64]{0,2,1:T(8,128)(2,1)S(1)}, u32[]{:S(2)}, u32[]{:S(2)}) %all-to-all-start.1) | async-done | bytes 524320 | tf_op jit(solution)/shard_map/all_to_all | solution.py:443
  (66 shorter events, 8.7 us)
Async XLA Ops:
  7.2 111.6 %copy-start = (bf16[2048,512]{1,0:T(8,128)(2,1)S(1)}, bf16[2048,512]{1,0:T(8,128)(2,1)}, u32[]{:S(2)}) copy-start(bf16[2048,512]{1,0:T(8,128)(2,1)} %param.28) | copy-start | bytes 6291460
  7.2 33.3 %copy-start.13 = (f32[256,32]{0,1:T(8,128)S(1)}, f32[256,32]{0,1:T(8,128)}, u32[]{:S(2)}) copy-start(f32[256,32]{0,1:T(8,128)} %param.20) | copy-start | bytes 98308
  7.2 33.4 %copy-start.14 = (f32[32,32]{1,0:T(8,128)S(1)}, f32[32,32]{1,0:T(8,128)}, u32[]{:S(2)}) copy-start(f32[32,32]{1,0:T(8,128)} %param.21) | copy-start | bytes 12292
  7.2 33.5 %copy-start.15 = (f32[32,32]{1,0:T(8,128)S(1)}, f32[32,32]{1,0:T(8,128)}, u32[]{:S(2)}) copy-start(f32[32,32]{1,0:T(8,128)} %param.22) | copy-start | bytes 12292
  7.2 33.5 %copy-start.12 = (f32[32,32,16]{1,2,0:T(8,128)S(1)}, f32[32,32,16]{1,2,0:T(8,128)}, u32[]{:S(2)}) copy-start(f32[32,32,16]{1,2,0:T(8,128)} %param.23) | copy-start | bytes 196612
  7.2 54.2 %all-gather.3.cloned.1.call-start = ((), (), s32[]{:S(2)}) async-start(), calls=%async_computation.2 | async-start | bytes 2621440 | tf_op jit(solution)/shard_map/all_gather | solution.py:417
  10.5 1.0 copy-start.1
  11.4 0.9 copy-start.4
  18.6 1.3 copy-start.7
  18.7 23.4 %copy-start.2 = (bf16[256,512]{1,0:T(8,128)(2,1)S(1)}, bf16[256,512]{1,0:T(8,128)(2,1)}, u32[]{:S(2)}) copy-start(bf16[256,512]{1,0:T(8,128)(2,1)} %rows_ref.1) | copy-start | bytes 786436
  18.8 23.4 %copy-start.9 = (f32[512]{0:T(512)S(1)}, f32[512]{0:T(512)}, u32[]{:S(2)}) copy-start(f32[512]{0:T(512)} %param.19) | copy-start | bytes 6148
  40.4 39.8 %all-gather.5.cloned.1.call-start = ((), (), s32[]{:S(2)}) async-start(), calls=%async_computation.3 | async-start | bytes 1310720 | tf_op jit(solution)/shard_map/all_gather | solution.py:431
  42.2 1.0 copy-start.5
  43.2 0.9 copy-start.6
  44.1 0.9 copy-start.8
  61.4 5.3 %copy-start.17 = (bf16[1,2048,1024]{2,1,0:T(8,128)(2,1)S(1)}, bf16[1,2048,1024]{2,1,0:T(8,128)(2,1)}, u32[]{:S(2)}) copy-start(bf16[1,2048,1024]{2,1,0:T(8,128)(2,1)} %param.34) | copy-start | bytes 12582916
  61.4 5.3 %copy-start.18 = (bf16[512,2048]{1,0:T(8,128)(2,1)S(1)}, bf16[512,2048]{1,0:T(8,128)(2,1)}, u32[]{:S(2)}) copy-start(bf16[512,2048]{1,0:T(8,128)(2,1)} %all-gather.3.cloned.1.call-done) | copy-start | bytes 6291460
  92.3 2.1 %collective-permute-start.1 = (bf16[512,512]{1,0:T(8,128)(2,1)}, bf16[512,512]{1,0:T(8,128)(2,1)S(1)}, u32[]{:S(2)}, u32[]{:S(2)}) collective-permute-start(bf16[512,512]{1,0:T(8,128)(2,1)} %get-tuple-element.21), channel_id=1, source_target_pairs={{0,1},{1,0},{2,3},{3,2},{4,5},{5,4},{6,7},{7,6},{8,9},{9,8},{10,11... | collective-permute-start | bytes 1572872 | tf_op jit(solution)/shard_map/ppermute | solution.py:360
  92.5 4.2 %collective-permute-start = (bf16[512,512]{1,0:T(8,128)(2,1)}, bf16[512,512]{1,0:T(8,128)(2,1)S(1)}, u32[]{:S(2)}, u32[]{:S(2)}) collective-permute-start(bf16[512,512]{1,0:T(8,128)(2,1)} %get-tuple-element.20), channel_id=1, source_target_pairs={{0,1},{1,0},{2,3},{3,2},{4,5},{5,4},{6,7},{7,6},{8,9},{9,8},{10,11... | collective-permute-start | bytes 1572872 | tf_op jit(solution)/shard_map/ppermute | solution.py:361
  96.4 14.4 %collective-permute-start.2 = (bf16[512,512]{1,0:T(8,128)(2,1)}, bf16[512,512]{1,0:T(8,128)(2,1)}, u32[]{:S(2)}, u32[]{:S(2)}) collective-permute-start(bf16[512,512]{1,0:T(8,128)(2,1)} %fusion.19), channel_id=1, source_target_pairs={{0,2},{2,0},{1,3},{3,1},{4,6},{6,4},{5,7},{7,5},{8,10},{10,8},{9,1... | collective-permute-start | bytes 1572872 | tf_op jit(solution)/shard_map/ppermute | solution.py:363
  96.7 21.9 %copy-start.16 = (f32[128,2]{0,1:T(2,128)S(1)}, f32[128,2]{0,1:T(2,128)}, u32[]{:S(2)}) copy-start(f32[128,2]{0,1:T(2,128)} %param.32) | copy-start | bytes 3076
  113.2 19.6 %all-to-all-start.1 = ((bf16[512,8,64]{0,2,1:T(8,128)(2,1)}), bf16[512,8,64]{0,2,1:T(8,128)(2,1)S(1)}, u32[]{:S(2)}, u32[]{:S(2)}) async-start(bf16[512,8,64]{0,2,1:T(8,128)(2,1)} %bitcast.17), calls=%async_computation.1 | async-start | bytes 1048576 | tf_op jit(solution)/shard_map/all_to_all | solution.py:443
  118.8 2.2 %copy-start.10 = (bf16[2048,512]{1,0:T(8,128)(2,1)S(1)}, bf16[2048,512]{1,0:T(8,128)(2,1)}, u32[]{:S(2)}) copy-start(bf16[2048,512]{1,0:T(8,128)(2,1)} %param.27) | copy-start | bytes 6291460
  118.8 2.2 %copy-start.11 = (bf16[256,2048]{1,0:T(8,128)(2,1)S(1)}, bf16[256,2048]{1,0:T(8,128)(2,1)}, u32[]{:S(2)}) copy-start(bf16[256,2048]{1,0:T(8,128)(2,1)} %all-gather.5.cloned.1.call-done) | copy-start | bytes 3145732
  (1 other events, 0.7 us)
Sparse Core Ops, SparseCore 0:
  40.5 20.7 all-gather.2
  63.5 16.6 all-gather.4
